TPU v7x, 512 devices: a whole 4x8x8 slice. The times are simulated.
512 devices in a mesh: kv: 128 (over z, y, core), tp: 4 (over x).
Axes of the slice: x: 4, y: 8, z: 8, core: 2. Of those that a mesh axis runs over, the one named last changes fastest.
Arguments:
- piece_tokens: bfloat16 [512, 2048], P('kv'), may hold values from -6 to 6
- decode_tokens: bfloat16 [128, 2048], P('kv'), may hold values from -6 to 6
- prompt_fill: int32 [1], replicated, may hold values from 16384 to 32256
- decode_fill: int32 [128], P('kv'), may hold values from 1 to 767, 49152 in all
- prompt_cache: bfloat16 [32768, 544], P('kv'), may hold values from -600 to 600
- decode_cache: bfloat16 [128, 768, 544], P('kv'), may hold values from -600 to 600
- input_gain: float32 [2048], replicated, may hold values from 0.1 to 1.9
- query_gain: float32 [768], replicated, may hold values from 0.1 to 1.9
- latent_gain: float32 [512], replicated, may hold values from 0.1 to 1.9
- query_down: bfloat16 [2048, 768], P(None, 'tp'), may hold values from -0.125 to 0.125
- latent_down: bfloat16 [2048, 512], P(None, 'tp'), may hold values from -0.125 to 0.125
- rope_down: bfloat16 [2048, 32], replicated, may hold values from -0.125 to 0.125
- query_up: bfloat16 [768, 1024], P(None, 'tp'), may hold values from -0.21875 to 0.21875
- qrope_up: bfloat16 [768, 512], P(None, 'tp'), may hold values from -0.21875 to 0.21875
- key_up: bfloat16 [16, 64, 512], P('tp'), may hold values from -0.25 to 0.25
- value_up: bfloat16 [16, 512, 64], P('tp'), may hold values from -4 to 4
- out_proj: bfloat16 [1024, 2048], P('tp'), may hold values from -4 to 4
Outputs:
- piece_out: bfloat16 [512, 2048], P('kv')
- decode_out: bfloat16 [128, 2048], P('kv')
- piece_rows: bfloat16 [512, 544], P('kv')
- decode_rows: bfloat16 [128, 544], P('kv')
Inputs may be any that keep to these rules, and one draw needn't show every extreme that they name: `prompt_fill`: the piece takes the 512 positions that follow the cache's filled positions. `decode_fill`: a decoding sequence's new token takes the position that follows its filled ones.
All inputs are finite; a program needn't handle non-finite values. No bound on the sum of `decode_fill` on one device may be relied on, other than what follows from the above.
Results may differ from a plain program's by a relative error of at most 0.035.
Values may be sent and summed in bfloat16 or wider, within the bound.
No kernel may reach another device: no remote copies, remote signals or barrier semaphores. Data moves between devices by JAX's collectives and lax.ppermute only.
A program may use at most 64 MiB of HBM per device.

v0:
```python
import jax
import jax.numpy as jnp
from jax import lax
from jax.sharding import PartitionSpec as P

NOPE = 64
ROPE = 32


NEG_FILL = -1e30
RMS_EPS = 1e-06
THETA = 10000.0


def laid_out(parts, dim):
    shape = list(parts.shape[1:])
    shape[dim] *= parts.shape[0]
    return jnp.moveaxis(parts, 0, dim).reshape(shape)


def gather_packed(arrays, axis, dims):
    flat = jnp.concatenate([a.reshape(-1) for a in arrays])
    lines, at, finished = (lax.all_gather(flat, axis), 0, [])
    for a, dim in zip(arrays, dims):
        parts = lines[:, at : at + a.size].reshape(-1, *a.shape)
        finished.append(laid_out(parts, dim))
        at += a.size
    return tuple(finished)


def sent_together(arrays, axis, split_dim, concat_dim, along):
    widths = [a.shape[along] for a in arrays]
    both = jnp.concatenate(arrays, axis=along)
    filled = lax.all_to_all(both, axis, split_axis=split_dim, concat_axis=concat_dim, tiled=True)
    return tuple(jnp.split(filled, [sum(widths[:k]) for k in range(1, len(widths))], axis=along))


def from_everyone(shard, axis):
    copies = jnp.broadcast_to(shard, (lax.axis_size(axis), *shard.shape))
    return lax.all_to_all(copies, axis, split_axis=0, concat_axis=0, tiled=True)


def over_copies(shard, axis):
    everything = from_everyone(shard, axis)
    return jnp.sum(everything.astype(jnp.float32), axis=0)


def rms_scale(values, gain_row):
    widened = values.astype(jnp.float32)
    scaled = (
        widened
        * lax.rsqrt(jnp.mean(widened * widened, axis=-1, keepdims=True) + RMS_EPS)
        * gain_row
    )
    return scaled.astype(jnp.bfloat16)


def rotate(values, places):
    half_width = values.shape[-1] // 2
    inverse = THETA ** (-jnp.arange(half_width, dtype=jnp.float32) / half_width)
    angles = places.astype(jnp.float32)[..., None] * inverse
    first_half = values[..., :half_width].astype(jnp.float32)
    second_half = values[..., half_width:].astype(jnp.float32)
    cosine = jnp.cos(angles)
    sine_part = jnp.sin(angles)
    return jnp.concatenate(
        [
            first_half * cosine - second_half * sine_part,
            first_half * sine_part + second_half * cosine,
        ],
        axis=-1,
    ).astype(jnp.bfloat16)


def make_queries(query_lat, places, query_up, qrope_up, key_up):
    row_count = query_lat.shape[0]
    head_count = key_up.shape[0]
    nope_part = (
        jnp.dot(query_lat, query_up, preferred_element_type=jnp.float32)
        .astype(jnp.bfloat16)
        .reshape(row_count, head_count, -1)
    )
    rope_raw = (
        jnp.dot(query_lat, qrope_up, preferred_element_type=jnp.float32)
        .astype(jnp.bfloat16)
        .reshape(row_count, head_count, -1)
    )
    turned = rotate(rope_raw, places[:, None])
    absorbed = jnp.einsum(
        "nhc,hcl->nhl", nope_part, key_up, preferred_element_type=jnp.float32
    ).astype(jnp.bfloat16)
    return (absorbed, turned)


def block_attend(absorbed, turned, key_rows, key_places, query_places, value_up):
    latent_width = value_up.shape[1]
    score_scale = (NOPE + ROPE) ** (-0.5)
    latent_keys = key_rows[:, :latent_width]
    scores = (
        jnp.einsum("nhl,sl->nhs", absorbed, latent_keys, preferred_element_type=jnp.float32)
        + jnp.einsum(
            "nhr,sr->nhs", turned, key_rows[:, latent_width:], preferred_element_type=jnp.float32
        )
    ) * score_scale
    allowed = key_places[None, None, :] <= query_places[:, None, None]
    scores = jnp.where(allowed, scores, NEG_FILL)
    local_peak = jnp.max(scores, axis=-1)
    exp_scores = jnp.where(allowed, jnp.exp(scores - local_peak[..., None]), 0.0)
    weight_sum = jnp.sum(exp_scores, axis=-1)
    weights = exp_scores.astype(jnp.bfloat16)
    mixed_rows = jnp.einsum("nhs,sl->nhl", weights, latent_keys, preferred_element_type=jnp.float32)
    partial_sum = jnp.einsum(
        "nhl,hlv->nhv", mixed_rows, value_up.astype(jnp.float32), precision=lax.Precision.HIGHEST
    )
    return (partial_sum, weight_sum, local_peak)


def insert_row(cache_rows, new_row, fill_one):
    return lax.dynamic_update_slice(cache_rows, new_row[None], (fill_one, jnp.zeros((), jnp.int32)))


def local(
    piece_tokens,
    decode_tokens,
    prompt_fill,
    decode_fill,
    prompt_cache,
    decode_cache,
    input_gain,
    query_gain,
    latent_gain,
    query_down,
    latent_down,
    rope_down,
    query_up,
    qrope_up,
    key_up,
    value_up,
    out_proj,
):
    kv_index = lax.axis_index("kv")
    piece_dev = piece_tokens.shape[0]
    shard_len = prompt_cache.shape[0]
    fill_start = prompt_fill[0]
    own_places = fill_start + kv_index * piece_dev + jnp.arange(piece_dev, dtype=jnp.int32)
    places = jnp.concatenate([own_places, decode_fill])
    tokens = jnp.concatenate([piece_tokens, decode_tokens], axis=0)
    normed = rms_scale(tokens, input_gain)
    query_comp = jnp.dot(normed, query_down, preferred_element_type=jnp.float32).astype(
        jnp.bfloat16
    )
    latent_comp = jnp.dot(normed, latent_down, preferred_element_type=jnp.float32).astype(
        jnp.bfloat16
    )
    query_comp, latent_comp = gather_packed((query_comp, latent_comp), "tp", (1, 1))
    query_lat = rms_scale(query_comp, query_gain)
    rope_raw = jnp.dot(normed, rope_down, preferred_element_type=jnp.float32).astype(jnp.bfloat16)
    new_rows = jnp.concatenate(
        [rms_scale(latent_comp, latent_gain), rotate(rope_raw, places)], axis=-1
    )
    piece_rows = new_rows[:piece_dev]
    decode_rows = new_rows[piece_dev:]
    decode_absorbed, decode_turned = make_queries(
        query_lat[piece_dev:], decode_fill, query_up, qrope_up, key_up
    )
    piece_latent, arrived = gather_packed((query_lat[:piece_dev], piece_rows), "kv", (0, 0))
    arrived_places = fill_start + jnp.arange(arrived.shape[0], dtype=jnp.int32)
    piece_absorbed, piece_turned = make_queries(
        piece_latent, arrived_places, query_up, qrope_up, key_up
    )
    piece_total = arrived.shape[0]
    query_places = fill_start + jnp.arange(piece_total, dtype=jnp.int32)
    zero_rows = jnp.zeros((shard_len, arrived.shape[1]), arrived.dtype)
    padded = jnp.concatenate([zero_rows, arrived, zero_rows], axis=0)
    offset = jnp.clip(kv_index * shard_len - fill_start + shard_len, 0, piece_total + shard_len)
    window = lax.dynamic_slice_in_dim(padded, offset, shard_len, 0)
    key_places = kv_index * shard_len + jnp.arange(shard_len, dtype=jnp.int32)
    fresh_rows = (key_places >= fill_start) & (key_places < fill_start + piece_total)
    key_rows = jnp.where(fresh_rows[:, None], window, prompt_cache)
    partial_sum, weight_sum, local_peak = block_attend(
        piece_absorbed, piece_turned, key_rows, key_places, query_places, value_up
    )
    all_parts, all_totals, all_peaks = sent_together(
        (partial_sum.reshape(1, piece_total, -1), weight_sum[None], local_peak[None]), "kv", 1, 0, 2
    )
    global_peak = jnp.max(all_peaks, axis=0)
    factor = jnp.exp(all_peaks - global_peak[None])
    merged = jnp.sum(all_parts.reshape(all_peaks.shape + (-1,)) * factor[..., None], axis=0)
    denominator = jnp.sum(all_totals * factor, axis=0)
    piece_value = (merged / denominator[..., None]).astype(jnp.bfloat16)
    decode_keys = jax.vmap(insert_row)(decode_cache, decode_rows, decode_fill)

    def attend_one(absorbed_one, turned_one, keys_one, fill_one):
        cache_places = jnp.arange(keys_one.shape[0], dtype=jnp.int32)
        return block_attend(
            absorbed_one[None], turned_one[None], keys_one, cache_places, fill_one[None], value_up
        )

    decode_part, decode_total, decode_peak = jax.vmap(attend_one)(
        decode_absorbed, decode_turned, decode_keys, decode_fill
    )
    decode_value = (decode_part[:, 0] / decode_total[:, 0, :, None]).astype(jnp.bfloat16)
    values = jnp.concatenate([piece_value, decode_value], axis=0)
    values = values.reshape(values.shape[0], -1)
    partial_value = jnp.dot(values, out_proj, preferred_element_type=jnp.float32).astype(
        jnp.bfloat16
    )
    summed = over_copies(partial_value, "tp").astype(jnp.float32).astype(jnp.bfloat16)
    return (summed[:piece_dev], summed[piece_dev:], piece_rows, decode_rows)


def solution(mesh):
    placed = (
        P("kv", None),
        P("kv", None),
        P(),
        P("kv"),
        P("kv", None),
        P("kv", None, None),
        P(),
        P(),
        P(),
        P(None, "tp"),
        P(None, "tp"),
        P(),
        P(None, "tp"),
        P(None, "tp"),
        P("tp", None, None),
        P("tp", None, None),
        P("tp", None),
    )
    return jax.shard_map(
        local,
        mesh=mesh,
        in_specs=placed,
        out_specs=(P("kv", None), P("kv", None), P("kv", None), P("kv", None)),
        check_vma=False,
    )
```

profile of v0, /device:TPU:8, one launch (start us, length us, event | category | flops | bytes accessed | tf_op | source)
XLA Modules:
  0.0 198.0 jit_solution(13090020181358731536)
XLA Ops:
  7.3 1.3 copy.110
  8.6 0.9 fusion.32
  9.6 1.5 convolution_convert_fusion.3
  11.5 1.3 dynamic-slice.11
  13.8 16.9 %all-reduce = bf16[6400]{0:T(1024)(128)(2,1)S(1)} all-reduce(bf16[6400]{0:T(1024)(128)(2,1)S(1)} %dynamic-update-slice.3), channel_id=2, replica_groups=mesh['kv'=128,'tp'=4] {'tp'}, use_global_device_ids=true, to_apply=%add | all-reduce | flops 6400 | bytes 25600
  32.4 1.1 convolution_convert_fusion.5
  35.2 0.9 copy.75
  37.6 2.0 %and_reduce_fusion = pred[]{:T(512)} fusion(s32[3]{0:T(128)S(1)} %copy-done.16, s32[1]{0:T(128)} %bitcast.22, s32[1]{0:T(128)} %bitcast.21, s32[1]{0:T(128)} %constant.80.clone.1), kind=kLoop, calls=%fused_computation.114 | loop fusion | flops 17 | bytes 25 | tf_op jit(solution)/shard_map/reduce.1
  39.6 1.2 broadcast_select_fusion
  41.0 1.6 scatter.4
  44.3 1.1 fusion.79
  45.6 75.0 %all-gather.5.cloned.1.call-done = bf16[128,1,5248]{2,1,0:T(2,128)(2,1)} async-done(((bf16[1,1,5248]{2,1,0:T(2,128)(2,1)}), bf16[128,1,5248]{2,1,0:T(2,128)(2,1)}) %all-gather.5.cloned.1.call-update) | async-done | bytes 1343504 | tf_op jit(solution)/shard_map/all_gather | solution.py:23
  120.6 1.9 copy.104
  123.6 2.1 %convolution_convert_fusion.1 = bf16[512,256]{0,1:T(8,128)(2,1)} fusion(bf16[512,768]{1,0:T(8,128)(2,1)S(1)} %reshape_reshape.6, bf16[768,256]{1,0:T(8,128)(2,1)} %param.31), kind=kOutput, calls=%fused_computation.13 | convolution fusion | flops 201457664 | bytes 1441792 | tf_op jit(solution)/shard_map/dot_general | solution.py:79
  126.5 0.9 fusion.22
  127.4 1.8 fusion.28
  129.1 3.2 %fusion.77 = (f32[512,4]{0,1:T(4,128)S(1)}, f32[512,4,256]{0,2,1:T(8,128)S(1)}) fusion(f32[512,4,256]{0,2,1:T(8,128)} %fusion.28, bf16[256,544]{1,0:T(8,128)(2,1)S(1)} %fusion.22, bf16[512,4,64]{0,2,1:T(8,128)(2,1)} %bitcast.107, bf16[4,64,512]{2,1,0:T(8,128)(2,1)} %param.33, pred[512,256]{0,1:T(8,128)(4,1)} %broadcast_compare_fusion), kind=kOutput, calls=%fused_computation.141 | convolution fusion | flops 674232320 | bytes 5120000 | tf_op jit(solution)/shard_map/nhl,sl->nhs/dot_general | solution.py:100
  132.4 1.7 fusion.13
  135.1 2.2 %fusion.78 = f32[4,512,64]{1,2,0:T(8,128)S(1)} fusion(f32[512,4,512]{2,0,1:T(8,128)S(1)} %fusion.13, bf16[4,512,64]{1,2,0:T(8,128)(2,1)S(1)} %copy-done.9), kind=kOutput, calls=%fused_computation.142 | convolution fusion | flops 805306368 | bytes 4980736 | tf_op jit(solution)/shard_map/nhl,hlv->nhv/dot_general | solution.py:112
  138.1 1.9 pad_maximum_fusion
  139.9 10.5 %all-to-all-start = ((f32[1,512,264]{2,0,1:T(1,128)}), f32[1,512,264]{2,0,1:T(1,128)S(1)}, u32[]{:S(2)}, u32[]{:S(2)}) async-start(f32[1,512,264]{2,0,1:T(1,128)} %pad_maximum_fusion), calls=%async_computation | async-start | bytes 1572864 | tf_op jit(solution)/shard_map/all_to_all | solution.py:34
  151.9 24.4 %all-to-all-done = f32[1,512,264]{2,0,1:T(1,128)S(1)} async-done(((f32[1,512,264]{2,0,1:T(1,128)}), f32[1,512,264]{2,0,1:T(1,128)S(1)}, u32[]{:S(2)}, u32[]{:S(2)}) %all-to-all-start) | async-done | bytes 540704 | tf_op jit(solution)/shard_map/all_to_all | solution.py:34
  176.2 1.9 reduce.21
  179.9 10.0 %all_to_all.17 = bf16[4,5,2048]{2,1,0:T(8,128)(2,1)S(1)} all-to-all(bf16[4,5,2048]{2,1,0:T(8,128)(2,1)S(1)} %broadcast_in_dim.94), channel_id=1, replica_groups=mesh['kv'=128,'tp'=4] {'tp'}, dimensions={0} | all-to-all | bytes 163840 | tf_op jit(solution)/shard_map/all_to_all | solution.py:40
  (122 shorter events, 14.1 us)
Async XLA Ops:
  7.2 172.4 %copy-start = (bf16[256,2048]{1,0:T(8,128)(2,1)S(1)}, bf16[256,2048]{1,0:T(8,128)(2,1)}, u32[]{:S(2)}) copy-start(bf16[256,2048]{1,0:T(8,128)(2,1)} %param.35) | copy-start | bytes 3145732
  7.2 28.9 %copy-start.17 = (s32[1,2]{1,0:T(1,128)S(1)}, s32[1,2]{1,0:T(1,128)}, u32[]{:S(2)}) copy-start(s32[1,2]{1,0:T(1,128)} %constant.83.clone.1) | copy-start | bytes 28
  7.2 30.4 %copy-start.16 = (s32[3]{0:T(128)S(1)}, s32[3]{0:T(128)}, u32[]{:S(2)}) copy-start(s32[3]{0:T(128)} %constant.84.clone.1) | copy-start | bytes 40
  7.2 4.0 %copy-start.10 = (bf16[4,2048]{1,0:T(4,128)(2,1)S(1)}, bf16[4,2048]{1,0:T(4,128)(2,1)}, u32[]{:S(2)}) copy-start(bf16[4,2048]{1,0:T(4,128)(2,1)} %param.19) | copy-start | bytes 49156
  7.2 4.0 %copy-start.11 = (bf16[1,2048]{1,0:T(2,128)(2,1)S(1)}, bf16[1,2048]{1,0:T(2,128)(2,1)}, u32[]{:S(2)}) copy-start(bf16[1,2048]{1,0:T(2,128)(2,1)} %param.20) | copy-start | bytes 12292
  7.2 27.9 %copy-start.8 = (bf16[256,544]{0,1:T(8,128)(2,1)S(1)}, bf16[256,544]{0,1:T(8,128)(2,1)}, u32[]{:S(2)}) copy-start(bf16[256,544]{0,1:T(8,128)(2,1)} %param.23) | copy-start | bytes 835588
  7.2 4.0 %copy-start.12 = (f32[2048]{0:T(1024)S(1)}, f32[2048]{0:T(1024)}, u32[]{:S(2)}) copy-start(f32[2048]{0:T(1024)} %param.25) | copy-start | bytes 24580
  7.3 27.1 %copy-start.14 = (f32[768]{0:T(1024)S(1)}, f32[768]{0:T(1024)}, u32[]{:S(2)}) copy-start(f32[768]{0:T(1024)} %param.26) | copy-start | bytes 9220
  7.3 26.4 %copy-start.15 = (f32[512]{0:T(512)S(1)}, f32[512]{0:T(512)}, u32[]{:S(2)}) copy-start(f32[512]{0:T(512)} %param.27) | copy-start | bytes 6148
  7.3 3.9 %copy-start.7 = (bf16[2048,128]{1,0:T(8,128)(2,1)S(1)}, bf16[2048,128]{1,0:T(8,128)(2,1)}, u32[]{:S(2)}) copy-start(bf16[2048,128]{1,0:T(8,128)(2,1)} %param.29) | copy-start | bytes 1572868
  7.3 113.3 %all-gather.5.cloned.1.call-start = ((), (), s32[]{:S(2)}) async-start(), calls=%async_computation.2 | async-start | bytes 2707968 | tf_op jit(solution)/shard_map/all_gather | solution.py:23
  8.6 34.0 %copy-start.3 = (bf16[768,256]{1,0:T(8,128)(2,1)S(1)}, bf16[768,256]{1,0:T(8,128)(2,1)}, u32[]{:S(2)}) copy-start(bf16[768,256]{1,0:T(8,128)(2,1)} %param.31) | copy-start | bytes 1179652
  8.6 34.3 %copy-start.6 = (bf16[768,128]{1,0:T(8,128)(2,1)S(1)}, bf16[768,128]{1,0:T(8,128)(2,1)}, u32[]{:S(2)}) copy-start(bf16[768,128]{1,0:T(8,128)(2,1)} %param.32) | copy-start | bytes 589828
  33.9 88.6 %copy-start.13 = (bf16[4,544]{1,0:T(4,128)(2,1)}, bf16[4,544]{1,0:T(4,128)(2,1)S(1)}, u32[]{:S(2)}) copy-start(bf16[4,544]{1,0:T(4,128)(2,1)S(1)} %slice.114) | copy-start | bytes 13060
  42.7 79.9 %copy-start.1 = (bf16[1,768,544]{1,2,0:T(8,128)(2,1)}, bf16[1,768,544]{1,2,0:T(8,128)(2,1)S(1)}, u32[]{:S(2)}) copy-start(bf16[1,768,544]{1,2,0:T(8,128)(2,1)S(1)} %scatter.4) | copy-start | bytes 2506756
  123.1 3.4 %copy-start.4 = (bf16[256,544]{1,0:T(8,128)(2,1)S(1)}, bf16[256,544]{1,0:T(8,128)(2,1)}, u32[]{:S(2)}) copy-start(bf16[256,544]{1,0:T(8,128)(2,1)} %copy.75) | copy-start | bytes 835588
  132.4 1.7 copy-start.5
  134.1 1.0 copy-start.9
  137.7 12.8 %copy-start.2 = (bf16[1,768,544]{1,2,0:T(8,128)(2,1)S(1)}, bf16[1,768,544]{1,2,0:T(8,128)(2,1)}, u32[]{:S(2)}) copy-start(bf16[1,768,544]{1,2,0:T(8,128)(2,1)} %copy-done.1) | copy-start | bytes 2506756
  139.9 36.3 %all-to-all-start = ((f32[1,512,264]{2,0,1:T(1,128)}), f32[1,512,264]{2,0,1:T(1,128)S(1)}, u32[]{:S(2)}, u32[]{:S(2)}) async-start(f32[1,512,264]{2,0,1:T(1,128)} %pad_maximum_fusion), calls=%async_computation | async-start | bytes 1572864 | tf_op jit(solution)/shard_map/all_to_all | solution.py:34
Sparse Core Ops, SparseCore 0:
  35.3 85.2 all-gather.4
where the time goes:
time: 199 us; the launch traced here: 198 us
  waiting for transfers between devices  99.4 us (50%)
  blocking collectives  26.9 us (14%)
  matrix products  17.1 us (9%)
  between operations  16.5 us (8%)
  local copies, waits for them, and re-layouts  15.1 us (8%)
  other arithmetic  12.4 us (6%)
  starting transfers between devices  10.6 us (5%)
    all_gather x1, waiting for transfers between devices, gather_packed(): lines, at, finished = (lax.all_gather(flat, axis), 0, [])  75 us
    all_to_all x1, waiting for transfers between devices, sent_together(): lax.all_to_all(both, axis, split_axis=split_dim, concat_axis=concat_dim,...  24.4 us
    unnamed x1, blocking collectives  16.9 us
    all_to_all x1, starting transfers between devices, sent_together(): lax.all_to_all(both, axis, split_axis=split_dim, concat_axis=concat_dim,...  10.5 us
    all_to_all x1, blocking collectives, from_everyone(): return lax.all_to_all(copies, axis, split_axis=0, concat_axis=0, tiled=True)  10 us
    unnamed x44, local copies, waits for them, and re-layouts  7.06 us
  transfers between devices with their start and end apart: 2, of which 2 were waited for; matrix products, arithmetic and copies ran while one was open for 6% of the time, Pallas kernels for 0%

commit v1 on v0

v1 whole, which is shorter than its diff:
```python
import jax
import jax.numpy as jnp
import numpy as np
from jax import lax
from jax.experimental import pallas as pl
from jax.experimental.pallas import tpu as pltpu
from jax.sharding import Mesh, PartitionSpec as P

NOPE = 64
ROPE = 32
NEG_FILL = -1e30
RMS_EPS = 1e-06
THETA = 10000.0
SCALE = (NOPE + ROPE) ** (-0.5)
TP = 4
PIECE_DEV = 4
BF = jnp.bfloat16
F32 = jnp.float32

GROUP = ("core",)
REST = ("z", "yh", "yl")
KV = ("z", "yh", "yl", "core")


def dot(a, b):
    return lax.dot_general(a, b, (((1,), (0,)), ((), ())), preferred_element_type=F32)


def dot_t(a, b):
    return lax.dot_general(a, b, (((1,), (1,)), ((), ())), preferred_element_type=F32)


def swap_matrix():
    rows = lax.broadcasted_iota(jnp.int32, (128, 128), 0)
    columns = lax.broadcasted_iota(jnp.int32, (128, 128), 1)
    return (rows == columns + jnp.where(columns % 32 < 16, 16, -16)).astype(BF)


def angle_tables(places):
    half = ROPE // 2
    inverse = THETA ** (-jnp.arange(half, dtype=F32) / half)
    angles = places.astype(F32)[:, None] * inverse
    cosine, sine = jnp.cos(angles), jnp.sin(angles)
    cos_table = jnp.concatenate([cosine, cosine] * TP, axis=-1)
    sin_table = jnp.concatenate([-sine, sine] * TP, axis=-1)
    return cos_table, sin_table


def turn(raw, cos_table, sin_table):
    swapped = dot(raw, swap_matrix())
    return (raw.astype(F32) * cos_table + swapped * sin_table).astype(BF)


def rms(values, gain):
    mean = jnp.mean(values * values, axis=-1, keepdims=True)
    return (values * lax.rsqrt(mean + RMS_EPS) * gain).astype(BF)


def head_lanes(width, rows):
    return lax.broadcasted_iota(jnp.int32, (rows, TP * width), 1) // width


def project_kernel(tokens, gain, query_t, latent, rope_t, cos_table, sin_table, out):
    normed = rms(tokens[...].astype(F32), gain[...])
    query = dot_t(normed, query_t[...])
    lat = dot(normed, latent[...])
    raw = dot_t(normed, rope_t[...]).astype(BF)
    raw = jnp.concatenate([raw.astype(F32)] * 4, axis=-1).astype(BF)
    turned = turn(raw, cos_table[...], sin_table[...])
    out[:, 0:192] = query.astype(BF)
    out[:, 256:384] = lat.astype(BF)
    out[:, 384:512] = turned


def rows_kernel(group, own, arrived, query_gain, latent_gain, query_out, rows_out, ropes_out):
    mine = own[0]
    parts = [arrived[mine * TP + p, :, 0:192].astype(F32) for p in range(TP)]
    query_out[...] = rms(jnp.concatenate(parts, axis=-1), query_gain[...])
    for j in range(group):
        parts = [arrived[j * TP + p, :, 256:384].astype(F32) for p in range(TP)]
        rows_out[j] = rms(jnp.concatenate(parts, axis=-1), latent_gain[...])
        ropes_out[j] = arrived[j * TP, :, 384:512]


def make_queries(query_lat, cos_table, sin_table, query_up, qrope_up):
    nope = dot(query_lat, query_up).astype(BF)
    raw = dot(query_lat, qrope_up).astype(BF)
    return nope, turn(raw, cos_table, sin_table)


def masked_to(values, width, head):
    lanes = head_lanes(width, values.shape[0])
    return jnp.where(lanes == head, values.astype(F32), 0.0).astype(BF)


def piece_kernel(group, rows, *refs):
    scalars, query_lat, cos_table, sin_table, query_up, qrope_up, key_up, value_up = refs[:8]
    caches = refs[8 : 8 + group]
    fresh, fresh_rope, out = refs[8 + group :]
    fill, own, rest = scalars[0], scalars[1], scalars[2]
    span = caches[0].shape[1]
    nope, turned = make_queries(
        query_lat[...], cos_table[...], sin_table[...], query_up[...], qrope_up[...]
    )
    fresh_keys = fresh[...]
    fresh_count = fresh_keys.shape[0]
    token = lax.broadcasted_iota(jnp.int32, (rows, fresh_count), 0)
    slot = lax.broadcasted_iota(jnp.int32, (rows, fresh_count), 1)
    query_rel = ((token // PIECE_DEV) * group + own) * PIECE_DEV + token % PIECE_DEV
    key_rel = (rest * group + slot // 8) * PIECE_DEV + slot % 8
    fresh_allowed = (slot % 8 < PIECE_DEV) & (key_rel <= query_rel)
    column = lax.broadcasted_iota(jnp.int32, (1, span), 1)
    keys = [c[0:512, :] for c in caches]
    ropes = [
        jnp.concatenate([c[512:544, :]] * TP, axis=0) for c in caches
    ]
    allowed = [column + scalars[3 + j] < fill for j in range(group)]
    values = jnp.zeros((rows, 256), F32)
    stats = jnp.zeros((rows, 128), F32)
    lane = lax.broadcasted_iota(jnp.int32, (rows, 128), 1)
    value_lanes = head_lanes(64, rows)
    for head in range(TP):
        absorbed = dot(masked_to(nope, 64, head), key_up[...]).astype(BF)
        turned_one = masked_to(turned, 32, head)
        scores = [
            jnp.where(ok, (dot(absorbed, k) + dot(turned_one, r)) * SCALE, NEG_FILL)
            for k, r, ok in zip(keys, ropes, allowed)
        ]
        extra = (dot_t(absorbed, fresh_keys) + dot_t(turned_one, fresh_rope[...])) * SCALE
        extra = jnp.where(fresh_allowed, extra, NEG_FILL)
        peak = jnp.max(extra, axis=-1, keepdims=True)
        for s in scores:
            peak = jnp.maximum(peak, jnp.max(s, axis=-1, keepdims=True))
        total = jnp.zeros((rows, 1), F32)
        mixed = jnp.zeros((rows, 512), F32)
        for s, k, ok in zip(scores, keys, allowed):
            weights = jnp.where(ok, jnp.exp(s - peak), 0.0)
            total = total + jnp.sum(weights, axis=-1, keepdims=True)
            mixed = mixed + dot_t(weights.astype(BF), k)
        weights = jnp.where(fresh_allowed, jnp.exp(extra - peak), 0.0)
        total = total + jnp.sum(weights, axis=-1, keepdims=True)
        mixed = mixed + dot(weights.astype(BF), fresh_keys)
        some = total > 0.0
        safe = jnp.where(some, total, 1.0)
        mixed = (mixed * (1.0 / safe)).astype(BF)
        level = jnp.where(some, peak + jnp.log(safe), NEG_FILL)
        values = jnp.where(value_lanes == head, dot_t(mixed, value_up[...]), values)
        rest_of = level
        for piece in range(3):
            part = rest_of.astype(BF).astype(F32)
            stats = jnp.where(lane == 3 * head + piece, part, stats)
            rest_of = rest_of - part
    out[:, 0:256] = values.astype(BF)
    out[:, 256:384] = stats.astype(BF)


def decode_kernel(scalars, query_lat, cos_table, sin_table, query_up, qrope_up, key_up,
                  value_up, cache, row, row_rope, out):
    fill = scalars[0]
    nope, turned = make_queries(
        query_lat[...], cos_table[...], sin_table[...], query_up[...], qrope_up[...]
    )
    nope, turned = nope.astype(F32)[0:1], turned.astype(F32)[0:1]
    head = lax.broadcasted_iota(jnp.int32, (8, 256), 0)
    nope = jnp.where(head_lanes(64, 8) == head, nope, 0.0).astype(BF)
    head = lax.broadcasted_iota(jnp.int32, (8, 128), 0)
    turned = jnp.where(head_lanes(32, 8) == head, turned, 0.0).astype(BF)
    absorbed = dot(nope, key_up[...]).astype(BF)
    keys = cache[0:512, :]
    ropes = jnp.concatenate([cache[512:544, :]] * TP, axis=0)
    span = cache.shape[1]
    allowed = lax.broadcasted_iota(jnp.int32, (8, span), 1) < fill
    scores = jnp.where(allowed, (dot(absorbed, keys) + dot(turned, ropes)) * SCALE, NEG_FILL)
    own = row[...].astype(F32)
    extra = jnp.sum(absorbed.astype(F32) * own, axis=-1, keepdims=True)
    extra += jnp.sum(turned.astype(F32) * row_rope[...].astype(F32), axis=-1, keepdims=True)
    extra = extra * SCALE
    peak = jnp.maximum(jnp.max(scores, axis=-1, keepdims=True), extra)
    weights = jnp.where(allowed, jnp.exp(scores - peak), 0.0)
    weight = jnp.exp(extra - peak)
    total = jnp.sum(weights, axis=-1, keepdims=True) + weight
    mixed = dot_t(weights.astype(BF), keys) + weight * own
    mixed = (mixed / total).astype(BF)
    projected = dot_t(mixed, value_up[...])
    head = lax.broadcasted_iota(jnp.int32, (8, 256), 0)
    projected = jnp.where(head_lanes(64, 8) == head, projected, 0.0)
    out[...] = jnp.sum(projected, axis=0, keepdims=True)


def merge_kernel(arrived, decode_value, out_proj, out):
    count = arrived.shape[0]
    source = lax.broadcasted_iota(jnp.int32, (128, 256), 0)
    target = lax.broadcasted_iota(jnp.int32, (128, 256), 1)
    spread = ((source // 3 == target // 64) & (source < 12)).astype(BF)
    level = dot(arrived[:, 256:384], spread).reshape(count // 8, 8, 256)
    values = arrived[:, 0:256].astype(F32).reshape(count // 8, 8, 256)
    top = jnp.max(level, axis=0)
    top = jnp.maximum(top, pltpu.roll(top, 4, 0))
    factor = jnp.exp(level - top[None])
    numer = jnp.sum(factor * values, axis=0)
    denom = jnp.sum(factor, axis=0)
    numer = numer + pltpu.roll(numer, 4, 0)
    denom = denom + pltpu.roll(denom, 4, 0)
    row = lax.broadcasted_iota(jnp.int32, (8, 256), 0)
    merged = jnp.where(row < 4, numer / denom, decode_value[...]).astype(BF)
    out[...] = dot(merged, out_proj[...]).astype(BF)


def call(kernel, out_shapes, operands, smem=(), flops=10**7):
    specs = [
        pl.BlockSpec(memory_space=pltpu.SMEM if k in smem else pltpu.VMEM)
        for k in range(len(operands))
    ]
    many = isinstance(out_shapes, (list, tuple))
    vmem = pl.BlockSpec(memory_space=pltpu.VMEM)
    size = sum(o.size * o.dtype.itemsize for o in operands)
    return pl.pallas_call(
        kernel,
        out_shape=out_shapes,
        in_specs=specs,
        out_specs=[vmem] * len(out_shapes) if many else vmem,
        cost_estimate=pl.CostEstimate(flops=flops, bytes_accessed=size, transcendentals=0),
    )(*operands)


def from_everyone(shard, axes):
    count = lax.axis_size(axes)
    copies = jnp.broadcast_to(shard, (count, *shard.shape))
    return lax.all_to_all(copies, axes, split_axis=0, concat_axis=0, tiled=True)


def local(
    piece_tokens,
    decode_tokens,
    prompt_fill,
    decode_fill,
    prompt_cache,
    decode_cache,
    input_gain,
    query_gain,
    latent_gain,
    query_down,
    latent_down,
    rope_down,
    query_up,
    qrope_up,
    key_up,
    value_up,
    out_proj,
):
    kv_index = lax.axis_index(KV)
    own = lax.axis_index(GROUP)
    rest = lax.axis_index(REST)
    group = lax.axis_size(GROUP)
    rest_count = lax.axis_size(REST)
    rows = rest_count * PIECE_DEV
    fill = prompt_fill[0]
    span = prompt_cache.shape[0]

    cache_t = prompt_cache.T
    caches = [cache_t, lax.ppermute(cache_t, "core", [(0, 1), (1, 0)])]
    bases = [kv_index * span, (rest * group + 1 - own) * span]

    step = jnp.arange(8, dtype=jnp.int32)
    places = jnp.where(step < PIECE_DEV, fill + kv_index * PIECE_DEV + step, decode_fill[0])
    cos_own, sin_own = angle_tables(places)
    tokens = jnp.concatenate([piece_tokens, decode_tokens, jnp.zeros((3, 2048), BF)], axis=0)
    packed = call(
        project_kernel,
        jax.ShapeDtypeStruct((8, 512), BF),
        (tokens, input_gain[None], query_down.T, latent_down, rope_down.T, cos_own, sin_own),
    )
    arrived = from_everyone(packed, GROUP + ("tp",))
    query_lat, new_rows, new_ropes = call(
        lambda *refs: rows_kernel(group, *refs),
        [
            jax.ShapeDtypeStruct((8, 768), BF),
            jax.ShapeDtypeStruct((group, 8, 512), BF),
            jax.ShapeDtypeStruct((group, 8, 128), BF),
        ],
        (own[None], arrived, query_gain[None], latent_gain[None]),
        smem=(0,),
    )
    own_rows = jnp.concatenate(
        [
            lax.dynamic_index_in_dim(new_rows, own, 0, keepdims=False),
            lax.dynamic_index_in_dim(new_ropes, own, 0, keepdims=False)[:, :ROPE],
        ],
        axis=-1,
    )

    piece_lat = from_everyone(query_lat[:PIECE_DEV], REST).reshape(rows, -1)

    key_flat = key_up.reshape(TP * NOPE, -1)
    value_flat = jnp.swapaxes(value_up, 1, 2).reshape(TP * 64, -1)
    decode_row = lax.dynamic_index_in_dim(new_rows, own, 0, keepdims=False)[4:5]
    decode_rope = lax.dynamic_index_in_dim(new_ropes, own, 0, keepdims=False)[4:5]
    decode_lat = jnp.broadcast_to(query_lat[4:5], query_lat.shape)
    decode_value = call(
        decode_kernel,
        jax.ShapeDtypeStruct((1, 256), F32),
        (
            decode_fill,
            decode_lat,
            cos_own[4:5],
            sin_own[4:5],
            query_up,
            qrope_up,
            key_flat,
            value_flat,
            decode_cache[0].T,
            decode_row,
            decode_rope,
        ),
        smem=(0,),
    )

    token = jnp.arange(rows, dtype=jnp.int32)
    class_places = fill + ((token // PIECE_DEV) * group + own) * PIECE_DEV + token % PIECE_DEV
    cos_class, sin_class = angle_tables(class_places)
    scalars = jnp.stack([fill, own, rest, *bases]).astype(jnp.int32)
    partial = call(
        lambda *refs: piece_kernel(group, rows, *refs),
        jax.ShapeDtypeStruct((rows, 384), BF),
        (
            scalars,
            piece_lat,
            cos_class,
            sin_class,
            query_up,
            qrope_up,
            key_flat,
            value_flat,
            *caches,
            new_rows.reshape(group * 8, -1),
            new_ropes.reshape(group * 8, -1),
        ),
        smem=(0,),
        flops=3 * 10**9,
    )
    returned = lax.all_to_all(
        partial.reshape(rest_count, PIECE_DEV, -1), REST, split_axis=0, concat_axis=0, tiled=True
    ).reshape(rows, -1)
    group_out = call(
        merge_kernel,
        jax.ShapeDtypeStruct((8, 2048), BF),
        (returned, decode_value, out_proj),
    )
    everyone = from_everyone(group_out, "tp")
    summed = jnp.sum(everyone.astype(F32), axis=0).astype(BF)
    return (summed[:PIECE_DEV], summed[PIECE_DEV : PIECE_DEV + 1], own_rows[:PIECE_DEV],
            own_rows[PIECE_DEV : PIECE_DEV + 1])


def solution(mesh):
    split = Mesh(mesh.devices.reshape(8, 4, 2, 2, TP), ("z", "yh", "yl", "core", "tp"))
    placed = (
        P(KV, None),
        P(KV, None),
        P(),
        P(KV),
        P(KV, None),
        P(KV, None, None),
        P(),
        P(),
        P(),
        P(None, "tp"),
        P(None, "tp"),
        P(),
        P(None, "tp"),
        P(None, "tp"),
        P("tp", None, None),
        P("tp", None, None),
        P("tp", None),
    )
    return jax.shard_map(
        local,
        mesh=split,
        in_specs=placed,
        out_specs=(P(KV, None), P(KV, None), P(KV, None), P(KV, None)),
        check_vma=False,
    )
```

time: 199 us -> 101 us (0.51)
  waiting for transfers between devices: 99.4 us -> 25.5 us
  blocking collectives: 26.9 us -> 0 us
  starting transfers between devices: 10.6 us -> 33.5 us
  matrix products: 17.1 us -> 0 us
  Pallas kernels: 0 us -> 16.5 us
  between operations: 16.5 us -> 2.07 us
  other arithmetic: 12.4 us -> 2.55 us
  local copies, waits for them, and re-layouts: 15.1 us -> 19.5 us
    all_gather x1 -> x0, waiting for transfers between devices: 75 us -> none  [gather_packed(): lines, at, finished = (lax.all_gather(flat, axis), 0, [])]
    all_to_all x1 -> x4, starting transfers between devices: 10.5 us -> 31 us  [the longest x3 25.8 us: from_everyone(): return lax.all_to_all(copies, axes, split_axis=0, concat_axis=0, tiled=True)]
    dot_general x17 -> x0, matrix products: 17.1 us -> none  [the longest x2 3.46 us: block_attend(): jnp.einsum('nhl,sl->nhs', absorbed, latent_keys, preferred_element_type=j...]
    unnamed x1 -> x0, blocking collectives: 16.9 us -> none
    pallas_call x0 -> x5, Pallas kernels: none -> 16.5 us  [call(): pl.pallas_call(kernel, out_shape=out_shapes, in_specs=specs, out_specs=[v...]
    all_to_all x1 -> x0, blocking collectives: 10 us -> none  [from_everyone(): return lax.all_to_all(copies, axis, split_axis=0, concat_axis=0, tiled=True)]
    unnamed x44 -> x18, local copies, waits for them, and re-layouts: 7.06 us -> 1.36 us
    slice x6 -> x8, local copies, waits for them, and re-layouts: 1.35 us -> 6.23 us  [the longest x1 1.26 us: local(): sin_own[4:5]]
  transfers between devices with their start and end apart: 2 -> 5, of which waited for: 2 -> 3; matrix products, arithmetic and copies ran while one was open for 6% -> 12% of each run, Pallas kernels for 0% -> 5%
where the time goes in v1:
time: 101 us; the launch traced here: 99.6 us
  starting transfers between devices  33.5 us (33%)
  waiting for transfers between devices  25.5 us (25%)
  local copies, waits for them, and re-layouts  19.5 us (19%)
  Pallas kernels  16.5 us (16%)
  other arithmetic  2.55 us (3%)
  between operations  2.07 us (2%)
    all_to_all x3, starting transfers between devices, from_everyone(): return lax.all_to_all(copies, axes, split_axis=0, concat_axis=0, tiled=True)  25.8 us
    all_to_all x3, waiting for transfers between devices, from_everyone(): return lax.all_to_all(copies, axes, split_axis=0, concat_axis=0, tiled=True)  18 us
    pallas_call x5, Pallas kernels, call(): pl.pallas_call(kernel, out_shape=out_shapes, in_specs=specs, out_specs=[v...  16.5 us
    all_to_all x1, waiting for transfers between devices, local(): lax.all_to_all(partial.reshape(rest_count, PIECE_DEV, -1), REST, split_ax...  7.43 us
    all_to_all x1, starting transfers between devices, local(): lax.all_to_all(partial.reshape(rest_count, PIECE_DEV, -1), REST, split_ax...  5.2 us
    broadcast_in_dim x3, local copies, waits for them, and re-layouts, from_everyone(): copies = jnp.broadcast_to(shard, (count, *shard.shape))  3.59 us
    ppermute x1, starting transfers between devices, local(): caches = [cache_t, lax.ppermute(cache_t, 'core', [(0, 1), (1, 0)])]  2.53 us
  transfers between devices with their start and end apart: 5, of which 3 were waited for; matrix products, arithmetic and copies ran while one was open for 12% of the time, Pallas kernels for 5%

profile of v1, /device:TPU:8, one launch (start us, length us, event | category | flops | bytes accessed | tf_op | source)
XLA Modules:
  0.0 99.6 jit_solution(15165043053133033300)
XLA Ops:
  4.2 2.7 %shard_map.192 = bf16[8,512]{1,0:T(8,128)(2,1)} custom-call(bf16[8,2048]{1,0:T(8,128)(2,1)} %maximum_maximum_fusion.tokens, f32[1,2048]{1,0:T(1,128)} %bitcast.41, bf16[192,2048]{1,0:T(8,128)(2,1)} %bitcast.33, bf16[2048,128]{1,0:T(8,128)(2,1)} %latent.1, bf16[32,2048]{1,0:T(8,128)(2,1)} %bitcast.38, f32[8,128]{1,0:T(8,128)} %concatenate.19.cos_table, ...), custom_call_target="tpu_custom_call" | custom-call | flops 10000000 | bytes 1490944 | tf_op jit(solution)/shard_map/pallas_call | solution.py:217
  6.9 1.3 %broadcast_in_dim.40 = bf16[8,8,512]{2,1,0:T(8,128)(2,1)} broadcast(bf16[8,512]{1,0:T(8,128)(2,1)} %shard_map.192), dimensions={1,2} | broadcast | bytes 73728 | tf_op jit(solution)/shard_map/broadcast_in_dim | solution.py:228
  8.2 4.3 %all-to-all-start = ((bf16[8,8,512]{2,1,0:T(8,128)(2,1)}), bf16[8,8,512]{2,1,0:T(8,128)(2,1)S(1)}, u32[]{:S(2)}, u32[]{:S(2)}) async-start(bf16[8,8,512]{2,1,0:T(8,128)(2,1)} %broadcast_in_dim.40), calls=%async_computation | async-start | bytes 131072 | tf_op jit(solution)/shard_map/all_to_all | solution.py:229
  12.5 2.5 %collective-permute-start = (bf16[544,256]{1,0:T(8,128)(2,1)S(1)}, bf16[544,256]{1,0:T(8,128)(2,1)S(1)}, u32[]{:S(2)}, u32[]{:S(2)}) collective-permute-start(bf16[544,256]{1,0:T(8,128)(2,1)S(1)} %bitcast.46), channel_id=1, source_target_pairs={{0,4},{4,0},{1,5},{5,1},{2,6},{6,2},{3,7},{7,3},{8,12},{12,8},{9,1... | collective-permute-start | bytes 835592 | tf_op jit(solution)/shard_map/ppermute | solution.py:261
  15.0 1.3 %slice.42.sin_table = f32[1,128]{1,0:T(1,128)} slice(f32[8,128]{1,0:T(8,128)} %concatenate.20.sin_table), slice={[4:5], [0:128]} | slice | bytes 1024 | tf_op jit(solution)/shard_map/slice | solution.py:306
  16.3 1.2 %slice.41.cos_table = f32[1,128]{1,0:T(1,128)} slice(f32[8,128]{1,0:T(8,128)} %concatenate.19.cos_table), slice={[4:5], [0:128]} | slice | bytes 1024 | tf_op jit(solution)/shard_map/slice | solution.py:305
  18.7 1.6 %shard_map.193 = (bf16[8,768]{1,0:T(8,128)(2,1)}, bf16[2,8,512]{2,1,0:T(8,128)(2,1)}, bf16[2,8,128]{2,1,0:T(8,128)(2,1)}) custom-call(s32[1]{0:T(128)} %bitcast.refs_0_, bf16[8,8,512]{2,1,0:T(8,128)(2,1)} %copy-done, f32[1,768]{1,0:T(1,128)} %broadcast_in_dim.41.refs_2_, f32[1,512]{1,0:T(1,128)} %bitcast.44), custom_call_target="tpu_custom_call" | custom-call | flops 10000000 | bytes 70660 | tf_op jit(solution)/shard_map/pallas_call | solution.py:217
  21.0 0.9 broadcast_in_dim.43
  21.9 16.6 %all-to-all-start.1 = ((bf16[64,4,768]{2,1,0:T(4,128)(2,1)}), bf16[64,4,768]{2,1,0:T(4,128)(2,1)S(1)}, u32[]{:S(2)}, u32[]{:S(2)}) async-start(bf16[64,4,768]{2,1,0:T(4,128)(2,1)} %broadcast_in_dim.43), calls=%async_computation.1 | async-start | bytes 786432 | tf_op jit(solution)/shard_map/all_to_all | solution.py:229
  39.0 1.0 concatenate.21.refs_2_
  40.0 0.9 concatenate.22.refs_3_
  41.5 0.7 slice_reduce_fusion
  42.8 12.7 %all-to-all-done.1 = bf16[64,4,768]{2,1,0:T(4,128)(2,1)S(1)} async-done(((bf16[64,4,768]{2,1,0:T(4,128)(2,1)}), bf16[64,4,768]{2,1,0:T(4,128)(2,1)S(1)}, u32[]{:S(2)}, u32[]{:S(2)}) %all-to-all-start.1) | async-done | bytes 393248 | tf_op jit(solution)/shard_map/all_to_all | solution.py:229
  55.5 0.8 reshape.71.refs_1_
  57.0 6.5 %shard_map.194 = bf16[256,384]{1,0:T(8,128)(2,1)} custom-call(s32[5]{0:T(128)} %stack.19.refs_0_, bf16[256,768]{1,0:T(8,128)(2,1)} %reshape.71.refs_1_, f32[256,128]{1,0:T(8,128)} %concatenate.21.refs_2_, f32[256,128]{1,0:T(8,128)} %concatenate.22.refs_3_, bf16[768,256]{1,0:T(8,128)(2,1)} %query_up.1, bf16[768,128]{1,0:T(8,128)(2,1)} %qrope_up.1, ...), custom_call_target="tpu_custom_call" | custom-call | flops 3000000000 | bytes 2347028 | tf_op jit(solution)/shard_map/pallas_call | solution.py:217
  63.5 1.7 %reshape.76 = bf16[64,4,384]{2,1,0:T(4,128)(2,1)} reshape(bf16[256,384]{1,0:T(8,128)(2,1)} %shard_map.194) | data formatting | bytes 393216 | tf_op jit(solution)/shard_map/reshape | solution.py:342
  65.2 5.2 %all-to-all-start.2 = ((bf16[64,4,384]{2,1,0:T(4,128)(2,1)}), bf16[64,4,384]{2,1,0:T(4,128)(2,1)S(1)}, u32[]{:S(2)}, u32[]{:S(2)}) async-start(bf16[64,4,384]{2,1,0:T(4,128)(2,1)} %reshape.76), calls=%async_computation.2 | async-start | bytes 393216 | tf_op jit(solution)/shard_map/all_to_all | solution.py:341
  71.6 3.2 %shard_map.195.decode_value = f32[1,256]{1,0:T(1,128)} custom-call(s32[1]{0:T(128)} %copy.23.scalars, bf16[8,768]{1,0:T(8,128)(2,1)} %broadcast_in_dim.45.query_lat, f32[1,128]{1,0:T(1,128)} %slice.41.cos_table, f32[1,128]{1,0:T(1,128)} %slice.42.sin_table, bf16[768,256]{1,0:T(8,128)(2,1)} %query_up.1, bf16[768,128]{1,0:T(8,128)(2,1)} %qrope_up.1, ...), custom_call_target="tpu_custom_call" | custom-call | flops 10000000 | bytes 1964292 | tf_op jit(solution)/shard_map/pallas_call | solution.py:217
  75.4 7.4 %all-to-all-done.2 = bf16[64,4,384]{2,1,0:T(4,128)(2,1)S(1)} async-done(((bf16[64,4,384]{2,1,0:T(4,128)(2,1)}), bf16[64,4,384]{2,1,0:T(4,128)(2,1)S(1)}, u32[]{:S(2)}, u32[]{:S(2)}) %all-to-all-start.2) | async-done | bytes 196640 | tf_op jit(solution)/shard_map/all_to_all | solution.py:341
  82.8 0.7 reshape.77.arrived
  83.6 2.5 %shard_map.196 = bf16[8,2048]{1,0:T(8,128)(2,1)} custom-call(bf16[256,384]{1,0:T(8,128)(2,1)} %reshape.77.arrived, f32[1,256]{1,0:T(1,128)} %shard_map.195.decode_value, bf16[256,2048]{1,0:T(8,128)(2,1)} %out_proj.1), custom_call_target="tpu_custom_call" | custom-call | flops 10000000 | bytes 1246208 | tf_op jit(solution)/shard_map/pallas_call | solution.py:217
  86.0 1.4 %broadcast_in_dim.46 = bf16[4,8,2048]{2,1,0:T(8,128)(2,1)} broadcast(bf16[8,2048]{1,0:T(8,128)(2,1)} %shard_map.196), dimensions={1,2} | broadcast | bytes 163840 | tf_op jit(solution)/shard_map/broadcast_in_dim | solution.py:228
  87.5 4.9 %all-to-all-start.3 = ((bf16[4,8,2048]{2,1,0:T(8,128)(2,1)}), bf16[4,8,2048]{2,1,0:T(8,128)(2,1)S(1)}, u32[]{:S(2)}, u32[]{:S(2)}) async-start(bf16[4,8,2048]{2,1,0:T(8,128)(2,1)} %broadcast_in_dim.46), calls=%async_computation.3 | async-start | bytes 262144 | tf_op jit(solution)/shard_map/all_to_all | solution.py:229
  93.0 5.4 %all-to-all-done.3 = bf16[4,8,2048]{2,1,0:T(8,128)(2,1)S(1)} async-done(((bf16[4,8,2048]{2,1,0:T(8,128)(2,1)}), bf16[4,8,2048]{2,1,0:T(8,128)(2,1)S(1)}, u32[]{:S(2)}, u32[]{:S(2)}) %all-to-all-start.3) | async-done | bytes 131104 | tf_op jit(solution)/shard_map/all_to_all | solution.py:229
  (44 shorter events, 10.2 us)
Async XLA Ops:
  2.8 0.8 copy-start.1
  2.8 0.8 copy-start.2
  4.2 8.3 %copy-start.7 = (bf16[256,544]{0,1:T(8,128)(2,1)S(1)}, bf16[256,544]{0,1:T(8,128)(2,1)}, u32[]{:S(2)}) copy-start(bf16[256,544]{0,1:T(8,128)(2,1)} %param.21) | copy-start | bytes 835588
  8.2 9.9 %all-to-all-start = ((bf16[8,8,512]{2,1,0:T(8,128)(2,1)}), bf16[8,8,512]{2,1,0:T(8,128)(2,1)S(1)}, u32[]{:S(2)}, u32[]{:S(2)}) async-start(bf16[8,8,512]{2,1,0:T(8,128)(2,1)} %broadcast_in_dim.40), calls=%async_computation | async-start | bytes 131072 | tf_op jit(solution)/shard_map/all_to_all | solution.py:229
  12.5 5.0 %copy-start.4 = (f32[768]{0:T(1024)S(1)}, f32[768]{0:T(1024)}, u32[]{:S(2)}) copy-start(f32[768]{0:T(1024)} %param.24) | copy-start | bytes 9220
  12.5 43.8 %collective-permute-start = (bf16[544,256]{1,0:T(8,128)(2,1)S(1)}, bf16[544,256]{1,0:T(8,128)(2,1)S(1)}, u32[]{:S(2)}, u32[]{:S(2)}) collective-permute-start(bf16[544,256]{1,0:T(8,128)(2,1)S(1)} %bitcast.46), channel_id=1, source_target_pairs={{0,4},{4,0},{1,5},{5,1},{2,6},{6,2},{3,7},{7,3},{8,12},{12,8},{9,1... | collective-permute-start | bytes 835592 | tf_op jit(solution)/shard_map/ppermute | solution.py:261
  18.1 0.6 copy-start
  21.9 33.6 %all-to-all-start.1 = ((bf16[64,4,768]{2,1,0:T(4,128)(2,1)}), bf16[64,4,768]{2,1,0:T(4,128)(2,1)S(1)}, u32[]{:S(2)}, u32[]{:S(2)}) async-start(bf16[64,4,768]{2,1,0:T(4,128)(2,1)} %broadcast_in_dim.43), calls=%async_computation.1 | async-start | bytes 786432 | tf_op jit(solution)/shard_map/all_to_all | solution.py:229
  41.5 0.7 copy-start.5
  56.3 0.7 copy-start.8
  65.2 5.2 %copy-start.3 = (bf16[2,8,512]{2,1,0:T(8,128)(2,1)S(1)}, bf16[2,8,512]{2,1,0:T(8,128)(2,1)}, u32[]{:S(2)}) copy-start(bf16[2,8,512]{2,1,0:T(8,128)(2,1)} %get-tuple-element.8) | copy-start | bytes 49156
  65.2 17.6 %all-to-all-start.2 = ((bf16[64,4,384]{2,1,0:T(4,128)(2,1)}), bf16[64,4,384]{2,1,0:T(4,128)(2,1)S(1)}, u32[]{:S(2)}, u32[]{:S(2)}) async-start(bf16[64,4,384]{2,1,0:T(4,128)(2,1)} %reshape.76), calls=%async_computation.2 | async-start | bytes 393216 | tf_op jit(solution)/shard_map/all_to_all | solution.py:341
  71.6 3.2 %copy-start.6 = (bf16[2,8,128]{2,1,0:T(8,128)(2,1)S(1)}, bf16[2,8,128]{2,1,0:T(8,128)(2,1)}, u32[]{:S(2)}) copy-start(bf16[2,8,128]{2,1,0:T(8,128)(2,1)} %get-tuple-element.9) | copy-start | bytes 12292
  87.5 10.9 %all-to-all-start.3 = ((bf16[4,8,2048]{2,1,0:T(8,128)(2,1)}), bf16[4,8,2048]{2,1,0:T(8,128)(2,1)S(1)}, u32[]{:S(2)}, u32[]{:S(2)}) async-start(bf16[4,8,2048]{2,1,0:T(8,128)(2,1)} %broadcast_in_dim.46), calls=%async_computation.3 | async-start | bytes 262144 | tf_op jit(solution)/shard_map/all_to_all | solution.py:229
